TPU v7x, 32 devices: a whole 2x2x4 slice. The times are simulated.
32 devices in a mesh: grp: 2 (over y), kv: 4 (over z), tp: 4 (over x, core).
Axes of the slice: x: 2, y: 2, z: 4, core: 2. Of those that a mesh axis runs over, the one named last changes fastest.
Arguments:
- hidden: bfloat16 [256, 4096], P('grp', 'kv'), parts along dimension 0, may hold values from -64 to 64
- norm_gain: bfloat16 [4096], replicated, may hold values from 0.099609375 to 1.8984375
- w_query: bfloat16 [4096, 2048], P('kv', 'tp'), may hold values from -0.09375 to 0.09375
- w_key: bfloat16 [4096, 2048], P('kv', 'tp'), may hold values from -0.09375 to 0.09375
- w_value: bfloat16 [4096, 2048], P('kv', 'tp'), may hold values from -0.09375 to 0.09375
- w_gate: bfloat16 [4096, 2048], P('kv', 'tp'), may hold values from -0.09375 to 0.09375
- w_decay: bfloat16 [4096, 16], P(None, 'tp'), may hold values from -0.09375 to 0.09375
- w_write: bfloat16 [4096, 16], P(None, 'tp'), may hold values from -0.09375 to 0.09375
- decay_rate: float32 [16], P('tp'), may hold values from 0.02 to 1
- head_gain: bfloat16 [128], replicated, may hold values from 0.099609375 to 1.8984375
- w_output: bfloat16 [2048, 4096], P('tp', 'kv'), may hold values from -0.125 to 0.125
- state: float32 [64, 16, 16384], P(('grp', 'kv'), 'tp'), parts along dimension 0, may hold values from -6 to 6
- prev_keys: bfloat16 [64, 4, 2048], P(('grp', 'kv'), None, 'tp'), parts along dimension 0, may hold values from -6 to 6
- prev_values: bfloat16 [64, 4, 2048], P(('grp', 'kv'), None, 'tp'), parts along dimension 0, may hold values from -6 to 6
- prev_decay: float32 [64, 4, 16], P(('grp', 'kv'), None, 'tp'), parts along dimension 0, may hold values from -1 to -0.02
- prev_write: float32 [64, 4, 16], P(('grp', 'kv'), None, 'tp'), parts along dimension 0, may hold values from 0.05 to 0.95
- accepted: int32 [64], P(('grp', 'kv')), parts along dimension 0, may hold values from 0 to 4
Outputs:
- mixed: bfloat16 [256, 4096], P('grp', 'kv'), parts along dimension 0
- state_out: float32 [64, 16, 16384], P(('grp', 'kv'), 'tp'), parts along dimension 0
There are 2 independent parts, one for each index of `grp`. A program takes and returns all parts, laid end to end along the dimension named above; an argument that names none is the same for every part. Nothing has to cross between parts.
All inputs are finite; a program needn't handle non-finite values.
Results may differ from a plain program's by a relative error of at most 0.0069.
Values may be sent and summed in bfloat16 or wider, within the bound.
A program may use at most 64 MiB of HBM per device.

v0:
```python
import functools

import jax
import jax.numpy as jnp
from jax import lax
from jax.experimental import pallas as pl
from jax.experimental.pallas import tpu as pltpu
from jax.sharding import PartitionSpec as P

EPSILON = 1e-06
F32 = jnp.float32
BF16 = jnp.bfloat16
MESH = pl.DeviceIdType.MESH
SMALL = 128
LOW = 16


def unit_rows(x):
    return x * lax.rsqrt(jnp.sum(x * x, axis=-1, keepdims=True) + EPSILON)


def dot(a, b):
    return jnp.dot(a, b, preferred_element_type=F32)


def dot_nt(a, b):
    return lax.dot_general(a, b, (((1,), (1,)), ((), ())), preferred_element_type=F32)


def kernel(
    n, tp, width_model,
    hidden_hbm, gain_ref, wq_hbm, wk_hbm, wv_hbm, wg_hbm, wd_ref, ww_ref, rate_ref, hgain_ref,
    wo_hbm, state_hbm, pk_ref, pv_ref, pd_ref, pw_ref, acc_ref,
    mixed_ref, sout_hbm,
    hid, wts, wo, send, recv, st, sb, newst, rows32, lbuf, ks, qs, dec, ho, gath,
    pf, pb, prx, pair, obuf,
    agg, recv2, ld_sem, st_sem, so_sem, rs_s, rs_r, r2_s, r2_r, ag_s, ag_r, p1_s, p1_r, p2_s, p2_r, p3_s, p3_r,
):
    me = lax.axis_index("kv")
    t = lax.axis_index("tp")
    core = lax.rem(t, 2)
    chip = t // 2
    chips = tp // 2
    partner = t + 1 - 2 * core
    tokens, local = hid.shape
    owned = tokens // n
    seqs = st.shape[0]
    heads = wd_ref.shape[0]
    width = wts.shape[2]
    dk = width // heads
    props = owned // seqs
    R = heads * owned

    kv_peers = [lax.rem(me + d, n) for d in range(1, n)]
    tp_peers = [lax.rem(t + 2 * k, tp) for k in range(1, chips)]

    parity = lax.rem(me, 2)
    neighbour = me + 1 - 2 * parity

    weights = (wk_hbm, wq_hbm, wv_hbm, wg_hbm)
    ld_h = pltpu.make_async_copy(hidden_hbm, hid, ld_sem.at[0])
    ld_h.start()
    ld_w = []
    for i, w in enumerate(weights):
        c = pltpu.make_async_copy(w, wts.at[i], ld_sem.at[1 + i])
        c.start()
        ld_w.append(c)
    barrier = pltpu.get_barrier_semaphore()
    for p in kv_peers:
        pl.semaphore_signal(barrier, inc=1, device_id={"kv": p}, device_id_type=MESH)
    for p in [partner] + tp_peers:
        pl.semaphore_signal(barrier, inc=1, device_id={"tp": p}, device_id_type=MESH)
    ld_s = []
    for s in range(seqs):
        c = pltpu.make_async_copy(state_hbm.at[s], st.at[s], st_sem.at[s])
        c.start()
        ld_s.append(c)
    ld_o = pltpu.make_async_copy(wo_hbm, wo, ld_sem.at[5])
    ld_o.start()

    ld_h.wait()
    offset = pl.multiple_of(me * local, local)
    wide = hid[...].astype(F32)
    table = gain_ref[...].astype(F32)
    lanes = table.shape[1]
    count = local // lanes
    gain = []
    for j in range(count):
        row = table[j : j + 1]
        for k in range(1, n):
            row = jnp.where(me == k, table[k * count + j : k * count + j + 1], row)
        gain.append(row)
    scaled = (wide * jnp.concatenate(gain, axis=1)).astype(BF16)
    squares = jnp.sum(wide * wide, axis=1, keepdims=True)
    wsmall = jnp.concatenate(
        [
            wd_ref[:, pl.ds(offset, local)].astype(F32),
            ww_ref[:, pl.ds(offset, local)].astype(F32),
            jnp.zeros((SMALL - 2 * heads, local), F32),
        ],
        axis=0,
    ).astype(BF16)
    small = dot_nt(scaled, wsmall)
    lane = lax.broadcasted_iota(jnp.int32, (tokens, SMALL), 1)
    small = small + jnp.where(lane == 2 * heads, squares, 0.0)
    high = small.astype(BF16).astype(F32)
    low = pltpu.roll(small - high, LOW, 1)
    send[:, :SMALL] = jnp.where(lane < LOW, high, low).astype(BF16)

    chunks = [(0, SMALL + width)] + [(SMALL + i * width, width) for i in range(1, 4)]
    rs = []
    for i in range(4):
        ld_w[i].wait()
        send[:, pl.ds(SMALL + i * width, width)] = dot(scaled, wts[i]).astype(BF16)
        if i == 0:
            pl.semaphore_wait(barrier, n - 1 + chips)
        lo, wd = chunks[i]
        group = []
        for j in range(n // 2):
            c = pltpu.make_async_remote_copy(
                src_ref=send.at[pl.ds(pl.multiple_of((2 * j + 1 - parity) * owned, owned), owned), pl.ds(lo, wd)],
                dst_ref=recv.at[j, :, pl.ds(lo, wd)],
                send_sem=rs_s.at[j, i],
                recv_sem=rs_r.at[j, i],
                device_id={"kv": neighbour},
                device_id_type=MESH,
            )
            c.start()
            group.append(c)
        rs.append(group)
    rs2 = []

    def relay(i):
        for c in rs[i]:
            c.wait()
        lo, wd = chunks[i]
        group = []
        for k in range(1, n // 2):
            target = lax.rem(me + 2 * k, n)
            rows = pl.ds(pl.multiple_of(target * owned, owned), owned)
            pairsum = send[rows, pl.ds(lo, wd)].astype(F32) + recv[target // 2, :, pl.ds(lo, wd)].astype(F32)
            agg[k - 1, :, pl.ds(lo, wd)] = pairsum.astype(BF16)
            c = pltpu.make_async_remote_copy(
                src_ref=agg.at[k - 1, :, pl.ds(lo, wd)],
                dst_ref=recv2.at[k - 1, :, pl.ds(lo, wd)],
                send_sem=r2_s.at[k - 1, i],
                recv_sem=r2_r.at[k - 1, i],
                device_id={"kv": target},
                device_id_type=MESH,
            )
            c.start()
            group.append(c)
        rs2.append(group)

    ri = lax.broadcasted_iota(jnp.int32, (R, R), 0)
    ci = lax.broadcasted_iota(jnp.int32, (R, R), 1)
    same = ri // props == ci // props
    lower = same & (ci <= ri)
    strict = same & (ci < ri)
    prow = ri % props
    per = heads * props
    src_row = ((ri // props) % heads) * owned + (ri // per) * props + ri % props
    perm = jnp.where(ci == src_row, 1.0, 0.0).astype(BF16)
    ek = lax.broadcasted_iota(jnp.int32, (dk, heads * dk), 0)
    ec = lax.broadcasted_iota(jnp.int32, (dk, heads * dk), 1)
    expand = jnp.where(ec // heads == ek, 1.0, 0.0).astype(BF16)
    lr = lax.broadcasted_iota(jnp.int32, (R, heads * dk), 0)
    lc = lax.broadcasted_iota(jnp.int32, (R, heads * dk), 1)
    lmask = (lr // props) % heads == lc % heads

    def spread_rows(xb):
        moved = dot(perm, xb).astype(BF16)
        return jnp.where(lmask, dot(moved, expand), 0.0).astype(BF16)

    def running(g):
        full = jnp.broadcast_to(g, (R, R))
        total = full
        for m in range(1, props):
            total = total + jnp.where(prow >= m, pltpu.roll(full, m, 0), 0.0)
        return full, total

    def decays(total):
        spread = total - total.T
        return jnp.where(lower, jnp.exp(jnp.where(lower, spread, 0.0)), 0.0)

    def coupling(kb, within, b):
        return jnp.where(strict, b * dot_nt(kb, kb) * within, 0.0).astype(BF16)

    def solve(a, rhs):
        u = rhs
        for _ in range(props - 1):
            u = rhs - dot(a, u.astype(BF16))
        return u

    def stack(get):
        return jnp.concatenate([get(h) for h in range(heads)], axis=0)

    def rows_of(ref):
        for s in range(seqs):
            rows32[pl.ds(s * props, props), :] = ref[s].astype(F32)
        return stack(lambda h: rows32[:, pl.ds(h * dk, dk)])

    kb = unit_rows(rows_of(pk_ref)).astype(BF16)
    values = rows_of(pv_ref)
    r16 = lax.broadcasted_iota(jnp.int32, (R, seqs), 0)
    c16 = lax.broadcasted_iota(jnp.int32, (R, seqs), 1)
    taken = ((r16 // props) % seqs == c16) & (r16 % props < acc_ref[...])
    pr = r16 % props
    hr = r16 // owned

    def column(ref):
        out = jnp.zeros((R, seqs), F32)
        for p in range(props):
            block = ref[p]
            for h in range(heads):
                out = jnp.where((pr == p) & (hr == h), block[h : h + 1, :], out)
        return jnp.sum(jnp.where(taken, out, 0.0), axis=1, keepdims=True)

    g = column(pd_ref)
    b = column(pw_ref)
    full, total = running(g)
    last = full
    tail = jnp.zeros((R, R), F32)
    for m in range(1, props):
        tail = tail + jnp.where(prow < props - m, pltpu.roll(full, R - m, 0), 0.0)
    within = decays(total)
    dec[...] = jnp.broadcast_to(jnp.exp((total + tail)[:, :1]), (R, dk))
    lbuf[0] = spread_rows(kb)
    for s in range(seqs):
        ld_s[s].wait()
        prod = dot(lbuf[0, pl.ds(s * per, per), :], st[s].astype(BF16))
        for h in range(heads):
            ks[pl.ds(h * owned + s * props, props), :] = prod[h * props : (h + 1) * props]
    u = solve(coupling(kb, within, b), b * (values - jnp.exp(total[:, :1]) * ks[...]))
    relay(0)
    u = dot(perm, (u * jnp.exp(tail[:, :1])).astype(BF16))
    relay(1)
    urow = lax.broadcasted_iota(jnp.int32, (R, dk), 0)
    lt = lbuf[0].T
    so = []
    for s in range(seqs):
        us = jnp.where(urow // per == s, u, 0.0).astype(BF16)
        pat = dec[pl.ds(s * props, heads, stride=owned), :]
        reps = 8 // heads if heads < 8 else 1
        pat = jnp.concatenate([pat] * reps, axis=0)
        old = st[s].reshape(heads * dk // pat.shape[0], pat.shape[0], dk)
        new = (old * pat[None]).reshape(heads * dk, dk) + dot(lt, us)
        newst[s] = new
        sb[s] = new.astype(BF16)
        c = pltpu.make_async_copy(newst.at[s], sout_hbm.at[s], so_sem.at[s])
        c.start()
        so.append(c)

    relay(2)
    relay(3)
    def arrive(chunk):
        for c in rs2[chunk]:
            c.wait()

    own = pl.ds(pl.multiple_of(me * owned, owned), owned)

    def summed(lo, wd):
        x = send[own, pl.ds(lo, wd)].astype(F32)
        x = x + recv[me // 2, :, pl.ds(lo, wd)].astype(F32)
        for k in range(1, n // 2):
            x = x + recv2[k - 1, :, pl.ds(lo, wd)].astype(F32)
        return x

    arrive(0)
    small = summed(0, SMALL)
    small = small + pltpu.roll(small, SMALL - LOW, 1)
    inverse = lax.rsqrt(small[:, 2 * heads : 2 * heads + 1] / width_model + EPSILON)
    small = small * inverse
    inv = jnp.concatenate([inverse] * heads, axis=0)
    sm = jnp.concatenate([small] * heads, axis=0)
    sl = lax.broadcasted_iota(jnp.int32, (R, SMALL), 1)
    sh = lax.broadcasted_iota(jnp.int32, (R, SMALL), 0) // owned
    apre = jnp.sum(jnp.where(sl == sh, sm, 0.0), axis=1, keepdims=True)
    bpre = jnp.sum(jnp.where(sl == sh + heads, sm, 0.0), axis=1, keepdims=True)
    hl = lax.broadcasted_iota(jnp.int32, (R, heads), 1)
    hh = lax.broadcasted_iota(jnp.int32, (R, heads), 0) // owned
    rate = jnp.sum(jnp.where(hl == hh, rate_ref[...], 0.0), axis=1, keepdims=True)
    softplus = jnp.maximum(apre, 0.0) + jnp.log1p(jnp.exp(-jnp.abs(apre)))
    g = -rate * softplus
    b = jax.nn.sigmoid(bpre)

    def projected(i):
        x = summed(SMALL + i * width, width)
        return stack(lambda h: x[:, h * dk : (h + 1) * dk]) * inv

    kb = unit_rows(projected(0)).astype(BF16)
    lbuf[0] = spread_rows(kb)
    full, total = running(g)
    within = decays(total)
    grow = jnp.exp(total[:, :1])
    couple = coupling(kb, within, b)
    arrive(1)
    qb = (unit_rows(projected(1)) * dk**-0.5).astype(BF16)
    lbuf[1] = spread_rows(qb)
    scores = (dot_nt(qb, kb) * within).astype(BF16)
    for s in range(seqs):
        lhs = jnp.concatenate(
            [lbuf[0, pl.ds(s * per, per), :], lbuf[1, pl.ds(s * per, per), :]], axis=0
        )
        prod = dot(lhs, sb[s])
        for h in range(heads):
            at = pl.ds(h * owned + s * props, props)
            ks[at, :] = prod[h * props : (h + 1) * props]
            qs[at, :] = prod[per + h * props : per + (h + 1) * props]
    arrive(2)
    u = solve(couple, b * (projected(2) - grow * ks[...]))
    read = grow * qs[...] + dot(scores, u.astype(BF16))
    normed = read * lax.rsqrt(jnp.mean(read * read, axis=-1, keepdims=True) + EPSILON)
    normed = normed * hgain_ref[...].astype(F32)
    arrive(3)
    gates = projected(3)
    normed = normed * (gates * jax.nn.sigmoid(gates))
    for h in range(heads):
        ho[:, pl.ds(h * dk, dk)] = normed[h * owned : (h + 1) * owned].astype(BF16)

    ag = []
    for d in range(n - 1, 0, -1):
        c = pltpu.make_async_remote_copy(
            src_ref=ho,
            dst_ref=gath.at[d - 1],
            send_sem=ag_s.at[d - 1],
            recv_sem=ag_r.at[d - 1],
            device_id={"kv": kv_peers[d - 1]},
            device_id_type=MESH,
        )
        c.start()
        ag.append(c)
    ag = ag[::-1]
    ld_o.wait()
    half = owned // 2
    first = []
    for d in range(n):
        if d:
            ag[d - 1].wait()
        block = dot(ho[...] if d == 0 else gath[d - 1], wo[...])
        for e in range(2):
            piece = block[e * half : (e + 1) * half]
            pf[d, e] = piece
            pb[d, e] = piece.astype(BF16)
        c = pltpu.make_async_remote_copy(
            src_ref=pb.at[d, 1 - core],
            dst_ref=prx.at[d],
            send_sem=p1_s.at[d],
            recv_sem=p1_r.at[d],
            device_id={"tp": partner},
            device_id_type=MESH,
        )
        c.start()
        first.append(c)
    second = []
    for d in range(n):
        first[d].wait()
        pair[d, chip] = (pf[d, core] + prx[d].astype(F32)).astype(BF16)
        group = []
        for k in range(1, chips):
            c = pltpu.make_async_remote_copy(
                src_ref=pair.at[d, chip],
                dst_ref=pair.at[d, chip],
                send_sem=p2_s.at[d, k - 1],
                recv_sem=p2_r.at[d, k - 1],
                device_id={"tp": tp_peers[k - 1]},
                device_id_type=MESH,
            )
            c.start()
            group.append(c)
        second.append(group)
    third = []
    for d in range(n):
        for c in second[d]:
            c.wait()
        x = pair[d, 0].astype(F32)
        for k in range(1, chips):
            x = x + pair[d, k].astype(F32)
        obuf[d, core] = x.astype(BF16)
        c = pltpu.make_async_remote_copy(
            src_ref=obuf.at[d, core],
            dst_ref=obuf.at[d, core],
            send_sem=p3_s.at[d],
            recv_sem=p3_r.at[d],
            device_id={"tp": partner},
            device_id_type=MESH,
        )
        c.start()
        third.append(c)
    for d in range(n):
        third[d].wait()
        mixed_ref[lax.rem(me - d + n, n)] = obuf[d]
    for c in so:
        c.wait()


def per_device(
    n, tp,
    hidden, norm_gain, w_query, w_key, w_value, w_gate, w_decay, w_write, decay_rate, head_gain,
    w_output, state, prev_keys, prev_values, prev_decay, prev_write, accepted,
):
    tokens, local = hidden.shape
    width = w_query.shape[1]
    heads = w_decay.shape[1]
    dk = width // heads
    seqs, props = prev_keys.shape[:2]
    owned = tokens // n
    half = owned // 2
    columns = w_output.shape[1]
    R = heads * owned
    total_width = SMALL + 4 * width
    chips = tp // 2
    view = state.reshape(seqs, heads, dk, dk).transpose(0, 2, 1, 3).reshape(seqs, dk * heads, dk)
    hbm = pl.BlockSpec(memory_space=pltpu.HBM)
    anyspace = pl.BlockSpec(memory_space=pl.ANY)
    vmem = pl.BlockSpec(memory_space=pltpu.VMEM)
    dma = pltpu.SemaphoreType.DMA
    mixed, state_out = pl.pallas_call(
        functools.partial(kernel, n, tp, norm_gain.shape[0]),
        out_shape=(
            pltpu.VMEM((n, 2, half, columns), BF16),
            pltpu.VMEM(view.shape, F32),
        ),
        in_specs=[hbm, vmem, hbm, hbm, hbm, hbm, vmem, vmem, vmem, vmem, hbm, hbm] + [vmem] * 5,
        out_specs=(vmem, anyspace),
        scratch_shapes=[
            pltpu.VMEM(hidden.shape, BF16),
            pltpu.VMEM((4,) + w_query.shape, BF16),
            pltpu.VMEM(w_output.shape, BF16),
            pltpu.VMEM((tokens, total_width), BF16),
            pltpu.VMEM((n // 2, owned, total_width), BF16),
            pltpu.VMEM(view.shape, F32),
            pltpu.VMEM(view.shape, BF16),
            pltpu.VMEM(view.shape, F32),
            pltpu.VMEM((owned, width), F32),
            pltpu.VMEM((2, R, width), BF16),
            pltpu.VMEM((R, dk), F32),
            pltpu.VMEM((R, dk), F32),
            pltpu.VMEM((R, dk), F32),
            pltpu.VMEM((owned, width), BF16),
            pltpu.VMEM((n - 1, owned, width), BF16),
            pltpu.VMEM((n, 2, half, columns), F32),
            pltpu.VMEM((n, 2, half, columns), BF16),
            pltpu.VMEM((n, half, columns), BF16),
            pltpu.VMEM((n, chips, half, columns), BF16),
            pltpu.VMEM((n, 2, half, columns), BF16),
            pltpu.VMEM((n // 2 - 1, owned, total_width), BF16),
            pltpu.VMEM((n // 2 - 1, owned, total_width), BF16),
            dma((6,)), dma((seqs,)), dma((seqs,)),
            dma((n // 2, 4)), dma((n // 2, 4)), dma((n // 2 - 1, 4)), dma((n // 2 - 1, 4)),
            dma((n - 1,)), dma((n - 1,)),
            dma((n,)), dma((n,)), dma((n, chips - 1)), dma((n, chips - 1)), dma((n,)), dma((n,)),
        ],
        compiler_params=pltpu.CompilerParams(
            collective_id=0, has_side_effects=True, vmem_limit_bytes=60 * 2**20
        ),
    )(
        hidden, norm_gain.reshape(-1, 128), w_query, w_key, w_value, w_gate, w_decay.T, w_write.T,
        decay_rate.reshape(1, -1), head_gain.reshape(1, -1), w_output, view, prev_keys, prev_values,
        prev_decay.transpose(1, 2, 0), prev_write.transpose(1, 2, 0), accepted.reshape(1, -1),
    )
    state_out = state_out.reshape(seqs, dk, heads, dk).transpose(0, 2, 1, 3)
    return mixed.reshape(tokens, columns), state_out.reshape(state.shape)


def solution(mesh):
    placed = (
        P("grp", "kv"),
        P(),
        P("kv", "tp"),
        P("kv", "tp"),
        P("kv", "tp"),
        P("kv", "tp"),
        P(None, "tp"),
        P(None, "tp"),
        P("tp"),
        P(),
        P("tp", "kv"),
        P(("grp", "kv"), "tp", None),
        P(("grp", "kv"), None, "tp"),
        P(("grp", "kv"), None, "tp"),
        P(("grp", "kv"), None, "tp"),
        P(("grp", "kv"), None, "tp"),
        P(("grp", "kv")),
    )
    return jax.shard_map(
        functools.partial(per_device, mesh.shape["kv"], mesh.shape["tp"]),
        mesh=mesh,
        in_specs=placed,
        out_specs=(P("grp", "kv"), P(("grp", "kv"), "tp", None)),
        check_vma=False,
    )
```

profile of v0, /device:TPU:0, one launch (start us, length us, event | category | flops | bytes accessed | tf_op | source)
XLA Modules:
  0.0 33.8 jit_solution(8786483266169491690)
XLA Ops:
  0.6 31.1 %shard_map.176 = (bf16[4,2,16,1024]{3,2,1,0:T(8,128)(2,1)S(1)}, f32[8,512,128]{2,1,0:T(8,128)S(1)}) custom-call(bf16[128,1024]{1,0:T(8,128)(2,1)} %hidden_hbm.1, bf16[32,128]{1,0:T(8,128)(2,1)} %bitcast.24, bf16[1024,512]{1,0:T(8,128)(2,1)} %wq_hbm.1, bf16[1024,512]{1,0:T(8,128)(2,1)} %wk_hbm.1, bf16[1024,512]{1,0:T(8,128)(2,1)} %wv_hbm.1, ...), custom_call_target="tpu_custom_call" | custom-call | tf_op jit(solution)/shard_map/pallas_call | solution.py:418
  31.7 0.7 %copy.23 = bf16[128,1024]{1,0:T(8,128)(2,1)} copy(bf16[128,1024]{1,0:T(8,128)(2,1)S(1)} %bitcast.20) | data formatting | bytes 524288
  32.4 1.3 %copy.24 = f32[8,4,16384]{2,1,0:T(4,128)} copy(f32[8,4,16384]{2,1,0:T(4,128)S(1)} %bitcast.19) | data formatting | bytes 4194304
where the time goes:
time: 34 us; the launch traced here: 33.8 us
  Pallas kernels  31.1 us (91%)
  local copies, waits for them, and re-layouts  2.02 us (6%)
  between operations  0.65 us (2%)
    pallas_call x1, Pallas kernels, per_device(): pl.pallas_call(functools.partial(kernel, n, tp, norm_gain.shape[0]), out_...  31.1 us
    unnamed x2, local copies, waits for them, and re-layouts  2.02 us

commit v1 on v0

--- a/solution.py
+++ b/solution.py
@@ -12,7 +12,7 @@
 BF16 = jnp.bfloat16
 MESH = pl.DeviceIdType.MESH
 SMALL = 128
-LOW = 16
+PACK = 32
 
 
 def unit_rows(x):
@@ -29,12 +29,14 @@
 
 def kernel(
     n, tp, width_model,
-    hidden_hbm, gain_ref, wq_hbm, wk_hbm, wv_hbm, wg_hbm, wd_ref, ww_ref, rate_ref, hgain_ref,
-    wo_hbm, state_hbm, pk_ref, pv_ref, pd_ref, pw_ref, acc_ref,
+    hidden_hbm, gain_hbm, wq_hbm, wk_hbm, wv_hbm, wg_hbm, wd_hbm, ww_hbm, rate_hbm, hgain_hbm,
+    wo_hbm, state_hbm, pk_hbm, pv_hbm, pd_hbm, pw_hbm, acc_hbm,
     mixed_ref, sout_hbm,
     hid, wts, wo, send, recv, st, sb, newst, rows32, lbuf, ks, qs, dec, ho, gath,
     pf, pb, prx, pair, obuf,
-    agg, recv2, ld_sem, st_sem, so_sem, rs_s, rs_r, r2_s, r2_r, ag_s, ag_r, p1_s, p1_r, p2_s, p2_r, p3_s, p3_r,
+    agg, recv2, spack, srecv,
+    gain_ref, wd_ref, ww_ref, rate_ref, hgain_ref, pk_ref, pv_ref, pd_ref, pw_ref, acc_ref,
+    ld_sem, sm_sem, st_sem, so_sem, rs_s, rs_r, r2_s, r2_r, sp_s, sp_r, ag_s, ag_r, p1_s, p1_r, p2_s, p2_r, p3_s, p3_r,
 ):
     me = lax.axis_index("kv")
     t = lax.axis_index("tp")
@@ -50,36 +52,45 @@
     dk = width // heads
     props = owned // seqs
     R = heads * owned
+    pairs = n // 2
+    packed = spack.shape[1]
+    groups = owned // packed
+    stride = SMALL // groups
 
     kv_peers = [lax.rem(me + d, n) for d in range(1, n)]
     tp_peers = [lax.rem(t + 2 * k, tp) for k in range(1, chips)]
-
     parity = lax.rem(me, 2)
     neighbour = me + 1 - 2 * parity
+    offset = pl.multiple_of(me * local, local)
+
+    def load(src, dst, sem):
+        c = pltpu.make_async_copy(src, dst, sem)
+        c.start()
+        return c
 
     weights = (wk_hbm, wq_hbm, wv_hbm, wg_hbm)
-    ld_h = pltpu.make_async_copy(hidden_hbm, hid, ld_sem.at[0])
-    ld_h.start()
-    ld_w = []
-    for i, w in enumerate(weights):
-        c = pltpu.make_async_copy(w, wts.at[i], ld_sem.at[1 + i])
-        c.start()
-        ld_w.append(c)
+    ld_h = load(hidden_hbm, hid, ld_sem.at[0])
+    ld_gain = load(gain_hbm, gain_ref, sm_sem.at[0])
     barrier = pltpu.get_barrier_semaphore()
     for p in kv_peers:
         pl.semaphore_signal(barrier, inc=1, device_id={"kv": p}, device_id_type=MESH)
     for p in [partner] + tp_peers:
         pl.semaphore_signal(barrier, inc=1, device_id={"tp": p}, device_id_type=MESH)
-    ld_s = []
-    for s in range(seqs):
-        c = pltpu.make_async_copy(state_hbm.at[s], st.at[s], st_sem.at[s])
-        c.start()
-        ld_s.append(c)
-    ld_o = pltpu.make_async_copy(wo_hbm, wo, ld_sem.at[5])
-    ld_o.start()
-
+    ld_w = [load(w, wts.at[i], ld_sem.at[1 + i]) for i, w in enumerate(weights)]
+    ld_d = load(wd_hbm.at[:, pl.ds(offset, local)], wd_ref, sm_sem.at[1])
+    ld_r = load(ww_hbm.at[:, pl.ds(offset, local)], ww_ref, sm_sem.at[2])
+    ld_prev = [
+        load(src, dst, sm_sem.at[3 + i])
+        for i, (src, dst) in enumerate(
+            [(pk_hbm, pk_ref), (pv_hbm, pv_ref), (pd_hbm, pd_ref), (pw_hbm, pw_ref), (acc_hbm, acc_ref)]
+        )
+    ]
+    ld_s = [load(state_hbm.at[s], st.at[s], st_sem.at[s]) for s in range(seqs)]
+    ld_late = [load(rate_hbm, rate_ref, sm_sem.at[8]), load(hgain_hbm, hgain_ref, sm_sem.at[9])]
+    ld_o = load(wo_hbm, wo, ld_sem.at[5])
+
+    ld_gain.wait()
     ld_h.wait()
-    offset = pl.multiple_of(me * local, local)
     wide = hid[...].astype(F32)
     table = gain_ref[...].astype(F32)
     lanes = table.shape[1]
@@ -92,57 +103,75 @@
         gain.append(row)
     scaled = (wide * jnp.concatenate(gain, axis=1)).astype(BF16)
     squares = jnp.sum(wide * wide, axis=1, keepdims=True)
+
+    cols = [pl.ds(i * width, width) for i in range(4)]
+    rs = []
+
+    def block(index):
+        return pl.ds(pl.multiple_of(index * owned, owned), owned)
+
+    def to_neighbour(k, i):
+        other = 2 * lax.rem(me // 2 + k, pairs) + 1 - parity
+        c = pltpu.make_async_remote_copy(
+            src_ref=send.at[block(other), cols[i]],
+            dst_ref=recv.at[k, :, cols[i]],
+            send_sem=rs_s.at[k, i],
+            recv_sem=rs_r.at[k, i],
+            device_id={"kv": neighbour},
+            device_id_type=MESH,
+        )
+        c.start()
+        return c
+
+    def project(i):
+        ld_w[i].wait()
+        send[:, cols[i]] = dot(scaled, wts[i]).astype(BF16)
+        if i == 0:
+            pl.semaphore_wait(barrier, n - 1 + chips)
+        rs.append([to_neighbour(k, i) for k in range(1, pairs)])
+
+    project(0)
+    ld_d.wait()
+    ld_r.wait()
     wsmall = jnp.concatenate(
-        [
-            wd_ref[:, pl.ds(offset, local)].astype(F32),
-            ww_ref[:, pl.ds(offset, local)].astype(F32),
-            jnp.zeros((SMALL - 2 * heads, local), F32),
-        ],
+        [wd_ref[...].astype(F32), ww_ref[...].astype(F32), jnp.zeros((SMALL - 2 * heads, local), F32)],
         axis=0,
     ).astype(BF16)
     small = dot_nt(scaled, wsmall)
     lane = lax.broadcasted_iota(jnp.int32, (tokens, SMALL), 1)
     small = small + jnp.where(lane == 2 * heads, squares, 0.0)
-    high = small.astype(BF16).astype(F32)
-    low = pltpu.roll(small - high, LOW, 1)
-    send[:, :SMALL] = jnp.where(lane < LOW, high, low).astype(BF16)
-
-    chunks = [(0, SMALL + width)] + [(SMALL + i * width, width) for i in range(1, 4)]
-    rs = []
-    for i in range(4):
-        ld_w[i].wait()
-        send[:, pl.ds(SMALL + i * width, width)] = dot(scaled, wts[i]).astype(BF16)
-        if i == 0:
-            pl.semaphore_wait(barrier, n - 1 + chips)
-        lo, wd = chunks[i]
+    small = small.reshape(n, groups, packed, SMALL)
+    tight = small[:, 0].reshape(n * packed, SMALL)
+    for j in range(1, groups):
+        tight = tight + pltpu.roll(small[:, j].reshape(n * packed, SMALL), j * stride, 1)
+    spack[...] = tight.reshape(n, packed, SMALL)
+    sp = []
+    for d in range(1, n):
+        c = pltpu.make_async_remote_copy(
+            src_ref=spack.at[kv_peers[d - 1]],
+            dst_ref=srecv.at[d - 1],
+            send_sem=sp_s.at[d - 1],
+            recv_sem=sp_r.at[d - 1],
+            device_id={"kv": kv_peers[d - 1]},
+            device_id_type=MESH,
+        )
+        c.start()
+        sp.append(c)
+    for i in range(1, 4):
+        project(i)
+
+    rs2 = []
+
+    def relay(i):
         group = []
-        for j in range(n // 2):
+        for k in range(1, pairs):
+            rs[i][k - 1].wait()
+            target = lax.rem(me + 2 * k, n)
+            pairsum = send[block(target), cols[i]].astype(F32) + recv[k, :, cols[i]].astype(F32)
+            agg[k - 1, :, cols[i]] = pairsum.astype(BF16)
             c = pltpu.make_async_remote_copy(
-                src_ref=send.at[pl.ds(pl.multiple_of((2 * j + 1 - parity) * owned, owned), owned), pl.ds(lo, wd)],
-                dst_ref=recv.at[j, :, pl.ds(lo, wd)],
-                send_sem=rs_s.at[j, i],
-                recv_sem=rs_r.at[j, i],
-                device_id={"kv": neighbour},
-                device_id_type=MESH,
-            )
-            c.start()
-            group.append(c)
-        rs.append(group)
-    rs2 = []
-
-    def relay(i):
-        for c in rs[i]:
-            c.wait()
-        lo, wd = chunks[i]
-        group = []
-        for k in range(1, n // 2):
-            target = lax.rem(me + 2 * k, n)
-            rows = pl.ds(pl.multiple_of(target * owned, owned), owned)
-            pairsum = send[rows, pl.ds(lo, wd)].astype(F32) + recv[target // 2, :, pl.ds(lo, wd)].astype(F32)
-            agg[k - 1, :, pl.ds(lo, wd)] = pairsum.astype(BF16)
-            c = pltpu.make_async_remote_copy(
-                src_ref=agg.at[k - 1, :, pl.ds(lo, wd)],
-                dst_ref=recv2.at[k - 1, :, pl.ds(lo, wd)],
+                src_ref=agg.at[k - 1, :, cols[i]],
+                dst_ref=recv2.at[k - 1, :, cols[i]],
                 send_sem=r2_s.at[k - 1, i],
                 recv_sem=r2_r.at[k - 1, i],
                 device_id={"kv": target},
@@ -200,6 +229,8 @@
             rows32[pl.ds(s * props, props), :] = ref[s].astype(F32)
         return stack(lambda h: rows32[:, pl.ds(h * dk, dk)])
 
+    for c in ld_prev:
+        c.wait()
     kb = unit_rows(rows_of(pk_ref)).astype(BF16)
     values = rows_of(pv_ref)
     r16 = lax.broadcasted_iota(jnp.int32, (R, seqs), 0)
@@ -211,15 +242,14 @@
     def column(ref):
         out = jnp.zeros((R, seqs), F32)
         for p in range(props):
-            block = ref[p]
+            piece = ref[p]
             for h in range(heads):
-                out = jnp.where((pr == p) & (hr == h), block[h : h + 1, :], out)
+                out = jnp.where((pr == p) & (hr == h), piece[h : h + 1, :], out)
         return jnp.sum(jnp.where(taken, out, 0.0), axis=1, keepdims=True)
 
     g = column(pd_ref)
     b = column(pw_ref)
     full, total = running(g)
-    last = full
     tail = jnp.zeros((R, R), F32)
     for m in range(1, props):
         tail = tail + jnp.where(prow < props - m, pltpu.roll(full, R - m, 0), 0.0)
@@ -231,12 +261,15 @@
         prod = dot(lbuf[0, pl.ds(s * per, per), :], st[s].astype(BF16))
         for h in range(heads):
             ks[pl.ds(h * owned + s * props, props), :] = prod[h * props : (h + 1) * props]
+    relay(0)
+    relay(1)
     u = solve(coupling(kb, within, b), b * (values - jnp.exp(total[:, :1]) * ks[...]))
-    relay(0)
     u = dot(perm, (u * jnp.exp(tail[:, :1])).astype(BF16))
-    relay(1)
     urow = lax.broadcasted_iota(jnp.int32, (R, dk), 0)
     lt = lbuf[0].T
+    relay(2)
+    relay(3)
+    direct = [to_neighbour(0, i) for i in range(4)]
     so = []
     for s in range(seqs):
         us = jnp.where(urow // per == s, u, 0.0).astype(BF16)
@@ -247,28 +280,30 @@
         new = (old * pat[None]).reshape(heads * dk, dk) + dot(lt, us)
         newst[s] = new
         sb[s] = new.astype(BF16)
-        c = pltpu.make_async_copy(newst.at[s], sout_hbm.at[s], so_sem.at[s])
-        c.start()
-        so.append(c)
-
-    relay(2)
-    relay(3)
-    def arrive(chunk):
-        for c in rs2[chunk]:
+        so.append(load(newst.at[s], sout_hbm.at[s], so_sem.at[s]))
+
+    own = block(me)
+
+    def summed(i):
+        x = send[own, cols[i]].astype(F32)
+        x = x + recv[0, :, cols[i]].astype(F32)
+        for k in range(1, pairs):
+            x = x + recv2[k - 1, :, cols[i]].astype(F32)
+        return x
+
+    def arrive(i):
+        for c in rs2[i]:
             c.wait()
-
-    own = pl.ds(pl.multiple_of(me * owned, owned), owned)
-
-    def summed(lo, wd):
-        x = send[own, pl.ds(lo, wd)].astype(F32)
-        x = x + recv[me // 2, :, pl.ds(lo, wd)].astype(F32)
-        for k in range(1, n // 2):
-            x = x + recv2[k - 1, :, pl.ds(lo, wd)].astype(F32)
-        return x
-
-    arrive(0)
-    small = summed(0, SMALL)
-    small = small + pltpu.roll(small, SMALL - LOW, 1)
+        direct[i].wait()
+
+    for c in sp + ld_late:
+        c.wait()
+    tight = spack[me]
+    for d in range(1, n):
+        tight = tight + srecv[d - 1]
+    small = jnp.concatenate(
+        [tight] + [pltpu.roll(tight, SMALL - j * stride, 1) for j in range(1, groups)], axis=0
+    )
     inverse = lax.rsqrt(small[:, 2 * heads : 2 * heads + 1] / width_model + EPSILON)
     small = small * inverse
     inv = jnp.concatenate([inverse] * heads, axis=0)
@@ -283,16 +318,17 @@
     softplus = jnp.maximum(apre, 0.0) + jnp.log1p(jnp.exp(-jnp.abs(apre)))
     g = -rate * softplus
     b = jax.nn.sigmoid(bpre)
-
-    def projected(i):
-        x = summed(SMALL + i * width, width)
-        return stack(lambda h: x[:, h * dk : (h + 1) * dk]) * inv
-
-    kb = unit_rows(projected(0)).astype(BF16)
-    lbuf[0] = spread_rows(kb)
     full, total = running(g)
     within = decays(total)
     grow = jnp.exp(total[:, :1])
+
+    def projected(i):
+        x = summed(i)
+        return stack(lambda h: x[:, h * dk : (h + 1) * dk]) * inv
+
+    arrive(0)
+    kb = unit_rows(projected(0)).astype(BF16)
+    lbuf[0] = spread_rows(kb)
     couple = coupling(kb, within, b)
     arrive(1)
     qb = (unit_rows(projected(1)) * dk**-0.5).astype(BF16)
@@ -318,28 +354,44 @@
     for h in range(heads):
         ho[:, pl.ds(h * dk, dk)] = normed[h * owned : (h + 1) * owned].astype(BF16)
 
+    left, right = me, n - 1 - me
+    most, least = jnp.maximum(left, right), jnp.minimum(left, right)
+    way = jnp.where(right >= left, 1, -1)
+
+    def ranked(k):
+        past = jnp.maximum(k - (most - least), 0)
+        far = jnp.where(k < most - least, most - k, least - past // 2)
+        return me + far * way * (1 - 2 * lax.rem(past, 2))
+
     ag = []
-    for d in range(n - 1, 0, -1):
+    for k in range(n - 1):
         c = pltpu.make_async_remote_copy(
             src_ref=ho,
-            dst_ref=gath.at[d - 1],
-            send_sem=ag_s.at[d - 1],
-            recv_sem=ag_r.at[d - 1],
-            device_id={"kv": kv_peers[d - 1]},
+            dst_ref=gath.at[me],
+            send_sem=ag_s.at[k],
+            recv_sem=ag_r.at[me],
+            device_id={"kv": ranked(k)},
             device_id_type=MESH,
         )
         c.start()
         ag.append(c)
-    ag = ag[::-1]
-    ld_o.wait()
+    source = [me] + [ranked(k) for k in range(n - 2, -1, -1)]
     half = owned // 2
-    first = []
-    for d in range(n):
+    first, second, third = [], [], []
+
+    def multiply(d):
         if d:
-            ag[d - 1].wait()
-        block = dot(ho[...] if d == 0 else gath[d - 1], wo[...])
+            pltpu.make_async_remote_copy(
+                src_ref=ho,
+                dst_ref=gath.at[source[d]],
+                send_sem=ag_s.at[0],
+                recv_sem=ag_r.at[source[d]],
+                device_id={"kv": source[d]},
+                device_id_type=MESH,
+            ).wait_recv()
+        part = dot(gath[source[d]] if d else ho[...], wo[...])
         for e in range(2):
-            piece = block[e * half : (e + 1) * half]
+            piece = part[e * half : (e + 1) * half]
             pf[d, e] = piece
             pb[d, e] = piece.astype(BF16)
         c = pltpu.make_async_remote_copy(
@@ -352,8 +404,8 @@
         )
         c.start()
         first.append(c)
-    second = []
-    for d in range(n):
+
+    def cross(d):
         first[d].wait()
         pair[d, chip] = (pf[d, core] + prx[d].astype(F32)).astype(BF16)
         group = []
@@ -369,8 +421,8 @@
             c.start()
             group.append(c)
         second.append(group)
-    third = []
-    for d in range(n):
+
+    def share(d):
         for c in second[d]:
             c.wait()
         x = pair[d, 0].astype(F32)
@@ -387,9 +439,26 @@
         )
         c.start()
         third.append(c)
-    for d in range(n):
+
+    def finish(d):
         third[d].wait()
-        mixed_ref[lax.rem(me - d + n, n)] = obuf[d]
+        mixed_ref[source[d]] = obuf[d]
+
+    ld_o.wait()
+    multiply(0)
+    cross(0)
+    for d in range(1, n):
+        multiply(d)
+        if d >= 2:
+            cross(d - 1)
+        share(d - 1) if d == 1 else None
+    cross(n - 1)
+    for d in range(1, n):
+        share(d)
+        finish(d - 1)
+    finish(n - 1)
+    for c in ag:
+        c.wait_send()
     for c in so:
         c.wait()
 
@@ -408,27 +477,32 @@
     half = owned // 2
     columns = w_output.shape[1]
     R = heads * owned
-    total_width = SMALL + 4 * width
     chips = tp // 2
+    packed = owned // (SMALL // PACK)
     view = state.reshape(seqs, heads, dk, dk).transpose(0, 2, 1, 3).reshape(seqs, dk * heads, dk)
     hbm = pl.BlockSpec(memory_space=pltpu.HBM)
     anyspace = pl.BlockSpec(memory_space=pl.ANY)
     vmem = pl.BlockSpec(memory_space=pltpu.VMEM)
     dma = pltpu.SemaphoreType.DMA
+    gain = norm_gain.reshape(-1, 128)
+    w_decay, w_write = w_decay.T, w_write.T
+    decay_rate, head_gain = decay_rate.reshape(1, -1), head_gain.reshape(1, -1)
+    prev_decay, prev_write = prev_decay.transpose(1, 2, 0), prev_write.transpose(1, 2, 0)
+    accepted = accepted.reshape(1, -1)
     mixed, state_out = pl.pallas_call(
         functools.partial(kernel, n, tp, norm_gain.shape[0]),
         out_shape=(
             pltpu.VMEM((n, 2, half, columns), BF16),
             pltpu.VMEM(view.shape, F32),
         ),
-        in_specs=[hbm, vmem, hbm, hbm, hbm, hbm, vmem, vmem, vmem, vmem, hbm, hbm] + [vmem] * 5,
+        in_specs=[hbm] * 17,
         out_specs=(vmem, anyspace),
         scratch_shapes=[
             pltpu.VMEM(hidden.shape, BF16),
             pltpu.VMEM((4,) + w_query.shape, BF16),
             pltpu.VMEM(w_output.shape, BF16),
-            pltpu.VMEM((tokens, total_width), BF16),
-            pltpu.VMEM((n // 2, owned, total_width), BF16),
+            pltpu.VMEM((tokens, 4 * width), BF16),
+            pltpu.VMEM((n // 2, owned, 4 * width), BF16),
             pltpu.VMEM(view.shape, F32),
             pltpu.VMEM(view.shape, BF16),
             pltpu.VMEM(view.shape, F32),
@@ -438,26 +512,38 @@
             pltpu.VMEM((R, dk), F32),
             pltpu.VMEM((R, dk), F32),
             pltpu.VMEM((owned, width), BF16),
-            pltpu.VMEM((n - 1, owned, width), BF16),
+            pltpu.VMEM((n, owned, width), BF16),
             pltpu.VMEM((n, 2, half, columns), F32),
             pltpu.VMEM((n, 2, half, columns), BF16),
             pltpu.VMEM((n, half, columns), BF16),
             pltpu.VMEM((n, chips, half, columns), BF16),
             pltpu.VMEM((n, 2, half, columns), BF16),
-            pltpu.VMEM((n // 2 - 1, owned, total_width), BF16),
-            pltpu.VMEM((n // 2 - 1, owned, total_width), BF16),
-            dma((6,)), dma((seqs,)), dma((seqs,)),
+            pltpu.VMEM((n // 2 - 1, owned, 4 * width), BF16),
+            pltpu.VMEM((n // 2 - 1, owned, 4 * width), BF16),
+            pltpu.VMEM((n, packed, SMALL), F32),
+            pltpu.VMEM((n - 1, packed, SMALL), F32),
+            pltpu.VMEM(gain.shape, BF16),
+            pltpu.VMEM((heads, local), BF16),
+            pltpu.VMEM((heads, local), BF16),
+            pltpu.VMEM(decay_rate.shape, F32),
+            pltpu.VMEM(head_gain.shape, BF16),
+            pltpu.VMEM(prev_keys.shape, BF16),
+            pltpu.VMEM(prev_values.shape, BF16),
+            pltpu.VMEM(prev_decay.shape, F32),
+            pltpu.VMEM(prev_write.shape, F32),
+            pltpu.VMEM(accepted.shape, jnp.int32),
+            dma((6,)), dma((10,)), dma((seqs,)), dma((seqs,)),
             dma((n // 2, 4)), dma((n // 2, 4)), dma((n // 2 - 1, 4)), dma((n // 2 - 1, 4)),
-            dma((n - 1,)), dma((n - 1,)),
+            dma((n - 1,)), dma((n - 1,)), dma((n - 1,)), dma((n,)),
             dma((n,)), dma((n,)), dma((n, chips - 1)), dma((n, chips - 1)), dma((n,)), dma((n,)),
         ],
         compiler_params=pltpu.CompilerParams(
             collective_id=0, has_side_effects=True, vmem_limit_bytes=60 * 2**20
         ),
     )(
-        hidden, norm_gain.reshape(-1, 128), w_query, w_key, w_value, w_gate, w_decay.T, w_write.T,
-        decay_rate.reshape(1, -1), head_gain.reshape(1, -1), w_output, view, prev_keys, prev_values,
-        prev_decay.transpose(1, 2, 0), prev_write.transpose(1, 2, 0), accepted.reshape(1, -1),
+        hidden, gain, w_query, w_key, w_value, w_gate, w_decay, w_write,
+        decay_rate, head_gain, w_output, view, prev_keys, prev_values,
+        prev_decay, prev_write, accepted,
     )
     state_out = state_out.reshape(seqs, dk, heads, dk).transpose(0, 2, 1, 3)
     return mixed.reshape(tokens, columns), state_out.reshape(state.shape)

time: 34 us -> 29.9 us (0.88)
  Pallas kernels: 31.1 us -> 27.1 us
    pallas_call x1, Pallas kernels: 31.1 us -> 27.1 us  [per_device(): pl.pallas_call(functools.partial(kernel, n, tp, norm_gain.shape[0]), out_...]
where the time goes in v1:
time: 29.9 us; the launch traced here: 29.8 us
  Pallas kernels  27.1 us (91%)
  local copies, waits for them, and re-layouts  2.02 us (7%)
  between operations  0.65 us (2%)
    pallas_call x1, Pallas kernels, per_device(): pl.pallas_call(functools.partial(kernel, n, tp, norm_gain.shape[0]), out_...  27.1 us
    unnamed x2, local copies, waits for them, and re-layouts  2.02 us

profile of v1, /device:TPU:0, one launch (start us, length us, event | category | flops | bytes accessed | tf_op | source)
XLA Modules:
  0.0 29.8 jit_solution(11821080780691638147)
XLA Ops:
  0.6 27.1 %shard_map.176 = (bf16[4,2,16,1024]{3,2,1,0:T(8,128)(2,1)S(1)}, f32[8,512,128]{2,1,0:T(8,128)S(1)}) custom-call(bf16[128,1024]{1,0:T(8,128)(2,1)} %hidden_hbm.1, bf16[32,128]{1,0:T(8,128)(2,1)} %bitcast.24, bf16[1024,512]{1,0:T(8,128)(2,1)} %wq_hbm.1, bf16[1024,512]{1,0:T(8,128)(2,1)} %wk_hbm.1, bf16[1024,512]{1,0:T(8,128)(2,1)} %wv_hbm.1, ...), custom_call_target="tpu_custom_call" | custom-call | tf_op jit(solution)/shard_map/pallas_call | solution.py:492
  27.8 0.7 %copy.23 = bf16[128,1024]{1,0:T(8,128)(2,1)} copy(bf16[128,1024]{1,0:T(8,128)(2,1)S(1)} %bitcast.20) | data formatting | bytes 524288
  28.5 1.3 %copy.24 = f32[8,4,16384]{2,1,0:T(4,128)} copy(f32[8,4,16384]{2,1,0:T(4,128)S(1)} %bitcast.19) | data formatting | bytes 4194304
